TPU v7x, 32 devices: a whole 2x2x4 slice. The times are simulated.
32 devices in a mesh: sp: 4 (over x, core), dp: 8 (over z, y).
Axes of the slice: x: 2, y: 2, z: 4, core: 2. Of those that a mesh axis runs over, the one named last changes fastest.
Arguments:
- tokens: bfloat16 [8, 1536, 2048], P('dp', 'sp'), may hold values from -6 to 6
- w_value: bfloat16 [2048, 1024], P('dp'), may hold values from -0.125 to 0.125
- w_gate: bfloat16 [2048, 1024], P('dp'), may hold values from -0.125 to 0.125
- conv_taps: bfloat16 [31, 1024], replicated, may hold values from -1 to 1
- norm_gain: bfloat16 [1024], replicated, may hold values from 0.099609375 to 1.8984375
- w_out: bfloat16 [1024, 2048], P(None, 'dp'), may hold values from -0.1875 to 0.1875
Outputs:
- mixed: bfloat16 [8, 1536, 2048], P('dp', 'sp')
All inputs are finite; a program needn't handle non-finite values.
Results may differ from a plain program's by a relative error of at most 0.013.
Values may be sent and summed in bfloat16 or wider, within the bound.
No kernel may reach another device: no remote copies, remote signals or barrier semaphores. Data moves between devices by JAX's collectives and lax.ppermute only.
A program may use at most 64 MiB of HBM per device.

v0:
```python
import jax
import jax.numpy as jnp
from jax import lax
from jax.sharding import PartitionSpec as P

EPSILON = 1e-06


def passed_along(x, axis, by):
    length = lax.axis_size(axis)
    pairs = [(i, i + by) for i in range(length) if 0 <= i + by < length]
    return lax.ppermute(x, axis, pairs)


def depthwise_conv(signal, local_taps, left_pad):
    kernel_form = jnp.transpose(local_taps)[:, None, :]
    result = lax.conv_general_dilated(
        signal[None],
        kernel_form,
        (1,),
        [(left_pad, 0)],
        dimension_numbers=("NCH", "OIH", "NCH"),
        feature_group_count=signal.shape[0],
        preferred_element_type=jnp.float32,
    )
    return result[0].astype(jnp.bfloat16)


def body(tokens, w_value, w_gate, conv_taps, norm_gain, w_out):
    seq_rows = tokens[0]
    tok_count = seq_rows.shape[0]
    kernel_len = conv_taps.shape[0]
    value_sum = jnp.einsum(
        "dc,td->ct",
        lax.all_gather(w_value, "dp", axis=0, tiled=True),
        seq_rows,
        preferred_element_type=jnp.float32,
    )
    gate_sum = jnp.einsum(
        "dc,td->ct",
        lax.all_gather(w_gate, "dp", axis=0, tiled=True),
        seq_rows,
        preferred_element_type=jnp.float32,
    )
    gated = (value_sum * jax.nn.sigmoid(gate_sum)).astype(jnp.bfloat16)
    last_rows = gated[:, tok_count - (kernel_len - 1) :]
    earlier = passed_along(last_rows, "sp", 1)
    extended = jnp.concatenate([earlier, gated], axis=1)
    conv_out = depthwise_conv(extended, conv_taps, 0)
    wide = conv_out.astype(jnp.float32)
    chan_mean = jnp.mean(wide, 0, keepdims=True)
    centred = wide - chan_mean
    chan_var = jnp.mean(centred * centred, 0, keepdims=True)
    normed = centred * lax.rsqrt(chan_var + EPSILON) * norm_gain.astype(jnp.float32)[:, None]
    activated = (normed * jax.nn.sigmoid(normed)).astype(jnp.bfloat16)
    projected = jnp.einsum(
        "ct,cd->td",
        activated,
        lax.all_gather(w_out, "dp", axis=1, tiled=True),
        preferred_element_type=jnp.float32,
    ).astype(jnp.bfloat16)
    return projected[None]


def solution(mesh):
    placed = (P("dp", "sp", None), P("dp", None), P("dp", None), P(), P(), P(None, "dp"))
    return jax.shard_map(
        body, mesh=mesh, in_specs=placed, out_specs=P("dp", "sp", None), check_vma=False
    )
```

profile of v0, /device:TPU:0, one launch (start us, length us, event | category | flops | bytes accessed | tf_op | source)
XLA Modules:
  0.0 246.4 jit_solution(6799378059922831921)
XLA Ops:
  6.5 0.0 copy-start
  6.5 0.0 all-gather.6.cloned.1.call-start
  6.5 0.7 all-gather.6.cloned.1.call-update
  7.3 0.0 all-gather.4.cloned.1.call-start
  7.3 0.7 all-gather.4.cloned.1.call-update
  8.0 0.0 all-gather.8.cloned.1.call-start
  8.1 0.7 all-gather.8.cloned.1.call-update
  8.7 76.3 %all-gather.6.cloned.1.call-done = bf16[2048,1024]{1,0:T(8,128)(2,1)} async-done(((bf16[256,1024]{1,0:T(8,128)(2,1)}), bf16[2048,1024]{1,0:T(8,128)(2,1)}) %all-gather.6.cloned.1.call-update) | async-done | bytes 4194320 | tf_op jit(solution)/shard_map/all_gather | solution.py:41
  85.0 0.0 copy-done
  85.0 4.0 %fusion.4 = f32[1024,384]{0,1:T(8,128)S(1)} fusion(bf16[2048,1024]{1,0:T(8,128)(2,1)} %all-gather.6.cloned.1.call-done, bf16[1,384,2048]{2,1,0:T(8,128)(2,1)S(1)} %copy-done), kind=kOutput, calls=%fused_computation.8 | convolution fusion | flops 1610612736 | bytes 7340032 | tf_op jit(solution)/shard_map/dc,td->ct/dot_general | solution.py:39
  89.0 0.0 copy-start.1
  89.0 69.5 %all-gather.4.cloned.1.call-done = bf16[2048,1024]{1,0:T(8,128)(2,1)} async-done(((bf16[256,1024]{1,0:T(8,128)(2,1)}), bf16[2048,1024]{1,0:T(8,128)(2,1)}) %all-gather.4.cloned.1.call-update) | async-done | bytes 4194320 | tf_op jit(solution)/shard_map/all_gather | solution.py:35
  158.5 4.1 %multiply_convert_fusion.1 = bf16[1024,384]{0,1:T(8,128)(2,1)S(1)} fusion(f32[1024,384]{0,1:T(8,128)S(1)} %fusion.4, bf16[2048,1024]{1,0:T(8,128)(2,1)} %all-gather.4.cloned.1.call-done, bf16[1,384,2048]{2,1,0:T(8,128)(2,1)S(1)} %copy-done), kind=kOutput, calls=%fused_computation.12 | convolution fusion | flops 1612578816 | bytes 8126464 | tf_op jit(solution)/shard_map/dc,td->ct/dot_general | solution.py:33
  162.6 1.3 collective-permute-start
  163.9 0.0 copy-done.1
  163.9 0.9 collective-permute-done
  164.8 0.2 maximum_bitcast_fusion
  165.0 0.1 pad
  165.0 0.2 reshape.17
  165.2 0.0 copy-start.2
  165.2 0.0 copy-start.3
  165.2 0.5 copy.12
  165.7 0.1 slice.7
  165.8 0.2 copy-done.2
  166.0 0.0 copy-done.3
  166.0 3.8 %fusion.17 = f32[8,52,1024]{2,0,1:T(8,128)S(1)} fusion(bf16[1024,1,7,30]{0,2,3,1:T(8,128)(2,1)S(1)} %slice.7, bf16[1024,1,8,52]{0,2,3,1:T(8,128)(2,1)S(1)} %copy.12, pred[8,52]{0,1:T(8,128)(4,1)S(1)} %copy-done.3, bf16[1024,1,31]{0,2,1:T(8,128)(2,1)S(1)} %bitcast.35), kind=kOutput, calls=%fused_computation.20 | convolution fusion | flops 31719424 | bytes 3049888 | tf_op jit(solution)/shard_map/conv_general_dilated | solution.py:17
  169.8 2.2 copy.14
  172.1 1.6 reshape.21
  173.7 0.2 slice_reduce_fusion
  173.8 0.3 multiply_reduce_fusion
  174.1 60.3 %all-gather.8.cloned.1.call-done = bf16[1024,2048]{1,0:T(8,128)(2,1)} async-done(((bf16[1024,256]{1,0:T(8,128)(2,1)}), bf16[1024,2048]{1,0:T(8,128)(2,1)}) %all-gather.8.cloned.1.call-update) | async-done | bytes 4194320 | tf_op jit(solution)/shard_map/all_gather | solution.py:59
  234.5 5.5 %fusion.1 = bf16[1,384,2048]{2,1,0:T(8,128)(2,1)} fusion(bf16[1024,2048]{1,0:T(8,128)(2,1)} %all-gather.8.cloned.1.call-done, f32[1,416,1024]{2,1,0:T(8,128)S(1)} %reshape.21, f32[1024]{0:T(1024)S(1)} %convert_element_type.26, f32[384]{0:T(512)S(1)} %add_rsqrt_fusion, f32[384]{0:T(512)S(1)} %broadcast_multiply_fusion), kind=kOutput, calls=%fused_computation.3 | convolution fusion | flops 1614544896 | bytes 7348224 | tf_op jit(solution)/shard_map/ct,cd->td/dot_general | solution.py:56
  (4 shorter events, 0.0 us)
Async XLA Ops:
  6.5 78.5 %copy-start = (bf16[1,384,2048]{2,1,0:T(8,128)(2,1)S(1)}, bf16[1,384,2048]{2,1,0:T(8,128)(2,1)}, u32[]{:S(2)}) copy-start(bf16[1,384,2048]{2,1,0:T(8,128)(2,1)} %param.6) | copy-start | bytes 4718596
  6.5 78.5 %all-gather.6.cloned.1.call-start = ((), (), s32[]{:S(2)}) async-start(), calls=%async_computation.1 | async-start | bytes 4718592 | tf_op jit(solution)/shard_map/all_gather | solution.py:41
  7.3 151.2 %all-gather.4.cloned.1.call-start = ((), (), s32[]{:S(2)}) async-start(), calls=%async_computation | async-start | bytes 4718592 | tf_op jit(solution)/shard_map/all_gather | solution.py:35
  8.0 226.4 %all-gather.8.cloned.1.call-start = ((), (), s32[]{:S(2)}) async-start(), calls=%async_computation.2 | async-start | bytes 4718592 | tf_op jit(solution)/shard_map/all_gather | solution.py:59
  89.0 74.9 %copy-start.1 = (bf16[1024]{0:T(1024)(128)(2,1)S(1)}, bf16[1024]{0:T(1024)(128)(2,1)}, u32[]{:S(2)}) copy-start(bf16[1024]{0:T(1024)(128)(2,1)} %param.10) | copy-start | bytes 6148
  162.6 2.2 collective-permute-start
  165.2 0.8 copy-start.2
  165.2 0.8 copy-start.3
Sparse Core Ops, SparseCore 0:
  9.5 75.5 all-gather.5
  87.1 71.3 all-gather.3
  160.5 73.8 all-gather.7
where the time goes:
time: 247 us; the launch traced here: 246 us
  waiting for transfers between devices  209 us (85%)
  matrix products  17.3 us (7%)
  between operations  13.2 us (5%)
  local copies, waits for them, and re-layouts  4.87 us (2%)
    all_gather x1, waiting for transfers between devices, body(): lax.all_gather(w_gate, 'dp', axis=0, tiled=True)  76.3 us
    all_gather x1, waiting for transfers between devices, body(): lax.all_gather(w_value, 'dp', axis=0, tiled=True)  69.5 us
    all_gather x1, waiting for transfers between devices, body(): lax.all_gather(w_out, 'dp', axis=1, tiled=True)  60.3 us
    dot_general x1, matrix products, body(): jnp.einsum('ct,cd->td', activated, lax.all_gather(w_out, 'dp', axis=1, ti...  5.46 us
  transfers between devices with their start and end apart: 4, of which 4 were waited for; matrix products, arithmetic and copies ran while one was open for 7% of the time, Pallas kernels for 0%

commit v1 on v0

--- a/solution.py
+++ b/solution.py
@@ -4,6 +4,20 @@
 from jax.sharding import PartitionSpec as P
 
 EPSILON = 1e-06
+
+
+def work_both_ways(x, axis, dim, make, out_dim):
+    ways, here, step = (lax.axis_size(axis), lax.axis_index(axis), x.shape[dim])
+    earlier, later = ([], [])
+    going_up = going_down = x
+    for far in range(ways // 2 + 1):
+        earlier.append(make(going_up, (here - far) % ways * step))
+        if 0 < far < ways - ways // 2:
+            later.append(make(going_down, (here + far) % ways * step))
+        going_up = lax.ppermute(going_up, axis, [(d, (d + 1) % ways) for d in range(ways)])
+        going_down = lax.ppermute(going_down, axis, [(d, (d - 1) % ways) for d in range(ways)])
+    line = jnp.concatenate([*earlier[::-1], *later], axis=out_dim)
+    return jnp.roll(line, (here - ways // 2) * earlier[0].shape[out_dim], axis=out_dim)
 
 
 def passed_along(x, axis, by):
@@ -53,11 +67,14 @@
     chan_var = jnp.mean(centred * centred, 0, keepdims=True)
     normed = centred * lax.rsqrt(chan_var + EPSILON) * norm_gain.astype(jnp.float32)[:, None]
     activated = (normed * jax.nn.sigmoid(normed)).astype(jnp.bfloat16)
-    projected = jnp.einsum(
-        "ct,cd->td",
-        activated,
-        lax.all_gather(w_out, "dp", axis=1, tiled=True),
-        preferred_element_type=jnp.float32,
+    projected = work_both_ways(
+        w_out,
+        "dp",
+        1,
+        lambda part, offset: jnp.einsum(
+            "ct,cd->td", activated, part, preferred_element_type=jnp.float32
+        ),
+        1,
     ).astype(jnp.bfloat16)
     return projected[None]
 

time: 247 us -> 238 us (0.964)
  waiting for transfers between devices: 209 us -> 175 us
  starting transfers between devices: 1.37 us -> 18.6 us
  matrix products: 17.3 us -> 21.9 us
    ppermute x0 -> x7, waiting for transfers between devices: none -> 63.4 us  [the longest x4 63.4 us: work_both_ways(): lax.ppermute(going_up, axis, [(d, (d + 1) % ways) for d in range(ways)])]
    all_gather x1 -> x0, waiting for transfers between devices: 60.3 us -> none  [body(): lax.all_gather(w_out, 'dp', axis=1, tiled=True)]
    all_gather x1, waiting for transfers between devices: 76.3 us -> 41.5 us  [body(): lax.all_gather(w_gate, 'dp', axis=0, tiled=True)]
    ppermute x0 -> x7, starting transfers between devices: none -> 17.2 us  [the longest x3 9.34 us: work_both_ways(): lax.ppermute(going_down, axis, [(d, (d - 1) % ways) for d in range(ways)])]
    dot_general x1 -> x8, matrix products: 5.46 us -> 8.38 us  [body(): jnp.einsum('ct,cd->td', activated, part, preferred_element_type=jnp.float32)]
  transfers between devices with their start and end apart: 4 -> 10, of which waited for: 4 -> 5; matrix products, arithmetic and copies ran while one was open for 7% -> 11% of each run, Pallas kernels for 0% -> 0%
where the time goes in v1:
time: 238 us; the launch traced here: 237 us
  waiting for transfers between devices  175 us (74%)
  matrix products  21.9 us (9%)
  starting transfers between devices  18.6 us (8%)
  between operations  13.8 us (6%)
  local copies, waits for them, and re-layouts  6.78 us (3%)
    all_gather x1, waiting for transfers between devices, body(): lax.all_gather(w_value, 'dp', axis=0, tiled=True)  68.5 us
    ppermute x4, waiting for transfers between devices, work_both_ways(): lax.ppermute(going_up, axis, [(d, (d + 1) % ways) for d in range(ways)])  63.4 us
    all_gather x1, waiting for transfers between devices, body(): lax.all_gather(w_gate, 'dp', axis=0, tiled=True)  41.5 us
    ppermute x3, starting transfers between devices, work_both_ways(): lax.ppermute(going_down, axis, [(d, (d - 1) % ways) for d in range(ways)])  9.34 us
    dot_general x8, matrix products, body(): jnp.einsum('ct,cd->td', activated, part, preferred_element_type=jnp.float32)  8.38 us
    ppermute x4, starting transfers between devices, work_both_ways(): lax.ppermute(going_up, axis, [(d, (d + 1) % ways) for d in range(ways)])  7.91 us
    dot_general x1, matrix products, body(): jnp.einsum('dc,td->ct', lax.all_gather(w_gate, 'dp', axis=0, tiled=True),...  5.12 us
  transfers between devices with their start and end apart: 10, of which 5 were waited for; matrix products, arithmetic and copies ran while one was open for 11% of the time, Pallas kernels for 0%

profile of v1, /device:TPU:0, one launch (start us, length us, event | category | flops | bytes accessed | tf_op | source)
XLA Modules:
  0.0 237.2 jit_solution(17859248095704365101)
XLA Ops:
  6.5 0.7 all-gather.5.cloned.1.call-update
  7.3 0.7 all-gather.3.cloned.1.call-update
  8.0 3.0 %collective-permute-start.1 = (bf16[1024,256]{1,0:T(8,128)(2,1)}, bf16[1024,256]{1,0:T(8,128)(2,1)S(1)}, u32[]{:S(2)}, u32[]{:S(2)}) collective-permute-start(bf16[1024,256]{1,0:T(8,128)(2,1)} %param.11), channel_id=1, source_target_pairs={{0,1},{1,2},{2,3},{3,4},{4,5},{5,6},{6,7},{7,0},{8,9},{9,10},{10,1... | collective-permute-start | bytes 1572872 | tf_op jit(solution)/shard_map/ppermute | solution.py:17
  11.1 3.1 %collective-permute-start.5 = (bf16[1024,256]{1,0:T(8,128)(2,1)}, bf16[1024,256]{1,0:T(8,128)(2,1)S(1)}, u32[]{:S(2)}, u32[]{:S(2)}) collective-permute-start(bf16[1024,256]{1,0:T(8,128)(2,1)} %param.11), channel_id=1, source_target_pairs={{0,7},{1,0},{2,1},{3,2},{4,3},{5,4},{6,5},{7,6},{8,15},{9,8},{10,9... | collective-permute-start | bytes 1572872 | tf_op jit(solution)/shard_map/ppermute | solution.py:18
  14.2 25.2 %collective-permute-done.1 = bf16[1024,256]{1,0:T(8,128)(2,1)S(1)} collective-permute-done((bf16[1024,256]{1,0:T(8,128)(2,1)}, bf16[1024,256]{1,0:T(8,128)(2,1)S(1)}, u32[]{:S(2)}, u32[]{:S(2)}) %collective-permute-start.1) | collective-permute-done | bytes 524320 | tf_op jit(solution)/shard_map/ppermute | solution.py:17
  39.4 2.4 %collective-permute-start.2 = (bf16[1024,256]{1,0:T(8,128)(2,1)S(1)}, bf16[1024,256]{1,0:T(8,128)(2,1)S(1)}, u32[]{:S(2)}, u32[]{:S(2)}) collective-permute-start(bf16[1024,256]{1,0:T(8,128)(2,1)S(1)} %collective-permute-done.1), channel_id=1, source_target_pairs={{0,1},{1,2},{2,3},{3,4},{4,5},{5,6},{6,7},{7,0},{8,9},{9,10},{10,1... | collective-permute-start | bytes 1572872 | tf_op jit(solution)/shard_map/ppermute | solution.py:17
  41.8 3.9 %collective-permute-start.6 = (bf16[1024,256]{1,0:T(8,128)(2,1)S(1)}, bf16[1024,256]{1,0:T(8,128)(2,1)}, u32[]{:S(2)}, u32[]{:S(2)}) collective-permute-start(bf16[1024,256]{1,0:T(8,128)(2,1)S(1)} %collective-permute-done.5), channel_id=1, source_target_pairs={{0,7},{1,0},{2,1},{3,2},{4,3},{5,4},{6,5},{7,6},{8,15},{9,8},{10,9... | collective-permute-start | bytes 1572872 | tf_op jit(solution)/shard_map/ppermute | solution.py:18
  45.7 25.1 %collective-permute-done.2 = bf16[1024,256]{1,0:T(8,128)(2,1)S(1)} collective-permute-done((bf16[1024,256]{1,0:T(8,128)(2,1)S(1)}, bf16[1024,256]{1,0:T(8,128)(2,1)S(1)}, u32[]{:S(2)}, u32[]{:S(2)}) %collective-permute-start.2) | collective-permute-done | bytes 524320 | tf_op jit(solution)/shard_map/ppermute | solution.py:17
  70.8 2.5 %collective-permute-start.3 = (bf16[1024,256]{1,0:T(8,128)(2,1)S(1)}, bf16[1024,256]{1,0:T(8,128)(2,1)}, u32[]{:S(2)}, u32[]{:S(2)}) collective-permute-start(bf16[1024,256]{1,0:T(8,128)(2,1)S(1)} %collective-permute-done.2), channel_id=1, source_target_pairs={{0,1},{1,2},{2,3},{3,4},{4,5},{5,6},{6,7},{7,0},{8,9},{9,10},{10,1... | collective-permute-start | bytes 1572872 | tf_op jit(solution)/shard_map/ppermute | solution.py:17
  73.3 41.5 %all-gather.5.cloned.1.call-done = bf16[2048,1024]{1,0:T(8,128)(2,1)} async-done(((bf16[256,1024]{1,0:T(8,128)(2,1)}), bf16[2048,1024]{1,0:T(8,128)(2,1)}) %all-gather.5.cloned.1.call-update) | async-done | bytes 4194320 | tf_op jit(solution)/shard_map/all_gather | solution.py:55
  114.8 5.1 %fusion.4 = f32[1024,384]{0,1:T(8,128)} fusion(bf16[2048,1024]{1,0:T(8,128)(2,1)} %all-gather.5.cloned.1.call-done, bf16[1,384,2048]{2,1,0:T(8,128)(2,1)S(1)} %copy-done), kind=kOutput, calls=%fused_computation.8 | convolution fusion | flops 1610612736 | bytes 7340032 | tf_op jit(solution)/shard_map/dc,td->ct/dot_general | solution.py:53
  119.9 68.5 %all-gather.3.cloned.1.call-done = bf16[2048,1024]{1,0:T(8,128)(2,1)} async-done(((bf16[256,1024]{1,0:T(8,128)(2,1)}), bf16[2048,1024]{1,0:T(8,128)(2,1)}) %all-gather.3.cloned.1.call-update) | async-done | bytes 4194320 | tf_op jit(solution)/shard_map/all_gather | solution.py:49
  188.5 4.5 %multiply_convert_fusion.1 = bf16[1024,384]{0,1:T(8,128)(2,1)S(1)} fusion(f32[1024,384]{0,1:T(8,128)} %fusion.4, bf16[2048,1024]{1,0:T(8,128)(2,1)} %all-gather.3.cloned.1.call-done, bf16[1,384,2048]{2,1,0:T(8,128)(2,1)S(1)} %copy-done), kind=kOutput, calls=%fused_computation.12 | convolution fusion | flops 1612578816 | bytes 8126464 | tf_op jit(solution)/shard_map/dc,td->ct/dot_general | solution.py:47
  193.1 1.3 collective-permute-start
  194.4 2.3 collective-permute-start.7
  196.8 0.2 maximum_bitcast_fusion
  197.2 0.5 copy.13
  197.9 3.9 %fusion.17 = f32[8,52,1024]{2,0,1:T(8,128)S(1)} fusion(bf16[1024,1,7,30]{0,2,3,1:T(8,128)(2,1)S(1)} %slice.7, bf16[1024,1,8,52]{0,2,3,1:T(8,128)(2,1)S(1)} %copy.13, pred[8,52]{0,1:T(8,128)(4,1)S(1)} %copy-done.10, bf16[1024,1,31]{0,2,1:T(8,128)(2,1)S(1)} %bitcast.49), kind=kOutput, calls=%fused_computation.20 | convolution fusion | flops 31719424 | bytes 3049888 | tf_op jit(solution)/shard_map/conv_general_dilated | solution.py:31
  201.8 2.2 copy.15
  204.0 1.6 reshape.21
  205.7 0.3 multiply_reduce_fusion
  206.1 0.6 multiply_convert_fusion
  206.7 13.1 %collective-permute-done.4 = bf16[1024,256]{1,0:T(8,128)(2,1)} collective-permute-done((bf16[1024,256]{1,0:T(8,128)(2,1)}, bf16[1024,256]{1,0:T(8,128)(2,1)}, u32[]{:S(2)}, u32[]{:S(2)}) %collective-permute-start.4) | collective-permute-done | bytes 524320 | tf_op jit(solution)/shard_map/ppermute | solution.py:17
  219.7 1.5 constant_dynamic-update-slice_fusion.15
  221.3 1.6 constant_dynamic-update-slice_fusion.14
  222.9 0.5 constant_dynamic-update-slice_fusion.13
  223.5 0.5 constant_dynamic-update-slice_fusion.12
  224.0 0.5 constant_dynamic-update-slice_fusion.11
  224.5 0.5 constant_dynamic-update-slice_fusion.10
  225.1 1.6 constant_dynamic-update-slice_fusion.9
  226.7 1.6 constant_dynamic-update-slice_fusion.8
  228.7 1.6 copy.16
  (47 shorter events, 1.1 us)
Async XLA Ops:
  6.5 108.3 %copy-start = (bf16[1,384,2048]{2,1,0:T(8,128)(2,1)S(1)}, bf16[1,384,2048]{2,1,0:T(8,128)(2,1)}, u32[]{:S(2)}) copy-start(bf16[1,384,2048]{2,1,0:T(8,128)(2,1)} %param.6) | copy-start | bytes 4718596
  6.5 108.3 %all-gather.5.cloned.1.call-start = ((), (), s32[]{:S(2)}) async-start(), calls=%async_computation.1 | async-start | bytes 4718592 | tf_op jit(solution)/shard_map/all_gather | solution.py:55
  7.3 181.2 %all-gather.3.cloned.1.call-start = ((), (), s32[]{:S(2)}) async-start(), calls=%async_computation | async-start | bytes 4718592 | tf_op jit(solution)/shard_map/all_gather | solution.py:49
  8.0 31.4 %collective-permute-start.1 = (bf16[1024,256]{1,0:T(8,128)(2,1)}, bf16[1024,256]{1,0:T(8,128)(2,1)S(1)}, u32[]{:S(2)}, u32[]{:S(2)}) collective-permute-start(bf16[1024,256]{1,0:T(8,128)(2,1)} %param.11), channel_id=1, source_target_pairs={{0,1},{1,2},{2,3},{3,4},{4,5},{5,6},{6,7},{7,0},{8,9},{9,10},{10,1... | collective-permute-start | bytes 1572872 | tf_op jit(solution)/shard_map/ppermute | solution.py:17
  11.1 30.7 %collective-permute-start.5 = (bf16[1024,256]{1,0:T(8,128)(2,1)}, bf16[1024,256]{1,0:T(8,128)(2,1)S(1)}, u32[]{:S(2)}, u32[]{:S(2)}) collective-permute-start(bf16[1024,256]{1,0:T(8,128)(2,1)} %param.11), channel_id=1, source_target_pairs={{0,7},{1,0},{2,1},{3,2},{4,3},{5,4},{6,5},{7,6},{8,15},{9,8},{10,9... | collective-permute-start | bytes 1572872 | tf_op jit(solution)/shard_map/ppermute | solution.py:18
  39.4 2.4 %copy-start.4 = (bf16[1024,256]{1,0:T(8,128)(2,1)}, bf16[1024,256]{1,0:T(8,128)(2,1)S(1)}, u32[]{:S(2)}) copy-start(bf16[1024,256]{1,0:T(8,128)(2,1)S(1)} %collective-permute-done.1) | copy-start | bytes 1572868
  39.4 31.4 %collective-permute-start.2 = (bf16[1024,256]{1,0:T(8,128)(2,1)S(1)}, bf16[1024,256]{1,0:T(8,128)(2,1)S(1)}, u32[]{:S(2)}, u32[]{:S(2)}) collective-permute-start(bf16[1024,256]{1,0:T(8,128)(2,1)S(1)} %collective-permute-done.1), channel_id=1, source_target_pairs={{0,1},{1,2},{2,3},{3,4},{4,5},{5,6},{6,7},{7,0},{8,9},{9,10},{10,1... | collective-permute-start | bytes 1572872 | tf_op jit(solution)/shard_map/ppermute | solution.py:17
  41.8 78.2 %copy-start.2 = (bf16[1024,256]{1,0:T(8,128)(2,1)}, bf16[1024,256]{1,0:T(8,128)(2,1)S(1)}, u32[]{:S(2)}) copy-start(bf16[1024,256]{1,0:T(8,128)(2,1)S(1)} %collective-permute-done.5) | copy-start | bytes 1572868
  41.8 152.6 %collective-permute-start.6 = (bf16[1024,256]{1,0:T(8,128)(2,1)S(1)}, bf16[1024,256]{1,0:T(8,128)(2,1)}, u32[]{:S(2)}, u32[]{:S(2)}) collective-permute-start(bf16[1024,256]{1,0:T(8,128)(2,1)S(1)} %collective-permute-done.5), channel_id=1, source_target_pairs={{0,7},{1,0},{2,1},{3,2},{4,3},{5,4},{6,5},{7,6},{8,15},{9,8},{10,9... | collective-permute-start | bytes 1572872 | tf_op jit(solution)/shard_map/ppermute | solution.py:18
  70.8 49.1 %copy-start.6 = (bf16[1024,256]{1,0:T(8,128)(2,1)}, bf16[1024,256]{1,0:T(8,128)(2,1)S(1)}, u32[]{:S(2)}) copy-start(bf16[1024,256]{1,0:T(8,128)(2,1)S(1)} %collective-permute-done.2) | copy-start | bytes 1572868
  70.8 125.9 %collective-permute-start.3 = (bf16[1024,256]{1,0:T(8,128)(2,1)S(1)}, bf16[1024,256]{1,0:T(8,128)(2,1)}, u32[]{:S(2)}, u32[]{:S(2)}) collective-permute-start(bf16[1024,256]{1,0:T(8,128)(2,1)S(1)} %collective-permute-done.2), channel_id=1, source_target_pairs={{0,1},{1,2},{2,3},{3,4},{4,5},{5,6},{6,7},{7,0},{8,9},{9,10},{10,1... | collective-permute-start | bytes 1572872 | tf_op jit(solution)/shard_map/ppermute | solution.py:17
  119.9 74.4 %copy-start.8 = (bf16[1024]{0:T(1024)(128)(2,1)S(1)}, bf16[1024]{0:T(1024)(128)(2,1)}, u32[]{:S(2)}) copy-start(bf16[1024]{0:T(1024)(128)(2,1)} %param.10) | copy-start | bytes 6148
  193.1 3.7 %collective-permute-start = (bf16[1024,30]{0,1:T(8,128)(2,1)S(1)}, bf16[1024,30]{0,1:T(8,128)(2,1)S(1)}, u32[]{:S(2)}, u32[]{:S(2)}) collective-permute-start(bf16[1024,30]{0,1:T(8,128)(2,1)S(1)} %slice.6), channel_id=1, source_target_pairs={{0,8},{8,16},{16,24},{1,9},{9,17},{17,25},{2,10},{10,18},{18,26},{... | collective-permute-start | bytes 184328 | tf_op jit(solution)/shard_map/ppermute | solution.py:26
  194.4 32.2 %collective-permute-start.7 = (bf16[1024,256]{1,0:T(8,128)(2,1)}, bf16[1024,256]{1,0:T(8,128)(2,1)}, u32[]{:S(2)}, u32[]{:S(2)}) collective-permute-start(bf16[1024,256]{1,0:T(8,128)(2,1)} %collective-permute-done.6), channel_id=1, source_target_pairs={{0,7},{1,0},{2,1},{3,2},{4,3},{5,4},{6,5},{7,6},{8,15},{9,8},{10,9... | collective-permute-start | bytes 1572872 | tf_op jit(solution)/shard_map/ppermute | solution.py:18
  196.8 23.0 %collective-permute-start.4 = (bf16[1024,256]{1,0:T(8,128)(2,1)}, bf16[1024,256]{1,0:T(8,128)(2,1)}, u32[]{:S(2)}, u32[]{:S(2)}) collective-permute-start(bf16[1024,256]{1,0:T(8,128)(2,1)} %collective-permute-done.3), channel_id=1, source_target_pairs={{0,1},{1,2},{2,3},{3,4},{4,5},{5,6},{6,7},{7,0},{8,9},{9,10},{10,1... | collective-permute-start | bytes 1572872 | tf_op jit(solution)/shard_map/ppermute | solution.py:17
  197.0 0.8 copy-start.9
  197.1 0.8 copy-start.10
  206.1 16.9 %copy-start.7 = (bf16[1024,256]{1,0:T(8,128)(2,1)S(1)}, bf16[1024,256]{1,0:T(8,128)(2,1)}, u32[]{:S(2)}) copy-start(bf16[1024,256]{1,0:T(8,128)(2,1)} %copy-done.6) | copy-start | bytes 1572868
  206.6 16.8 %copy-start.5 = (bf16[1024,256]{1,0:T(8,128)(2,1)S(1)}, bf16[1024,256]{1,0:T(8,128)(2,1)}, u32[]{:S(2)}) copy-start(bf16[1024,256]{1,0:T(8,128)(2,1)} %copy-done.4) | copy-start | bytes 1572868
  221.3 2.7 %copy-start.1 = (bf16[1024,256]{1,0:T(8,128)(2,1)S(1)}, bf16[1024,256]{1,0:T(8,128)(2,1)}, u32[]{:S(2)}) copy-start(bf16[1024,256]{1,0:T(8,128)(2,1)} %param.11) | copy-start | bytes 1572868
  222.9 1.6 copy-start.3
Sparse Core Ops, SparseCore 0:
  9.5 105.3 all-gather.4
  116.9 71.5 all-gather.2
